TPU v7x, 32 devices: a whole 2x2x4 slice. The times are simulated.
32 devices in a mesh: sp: 4 (over z), tp: 8 (over y, x, core).
Axes of the slice: x: 2, y: 2, z: 4, core: 2. Of those that a mesh axis runs over, the one named last changes fastest.
Arguments:
- target: bfloat16 [512, 2048], P('sp'), may hold values from -6 to 6
- source: bfloat16 [1024, 2048], P(('sp', 'tp')), may hold values from -6 to 6
- cotangent: bfloat16 [512, 2048], P('sp'), may hold values from -6 to 6
- target_gain: float32 [2048], replicated, may hold values from 0.1 to 1.9
- source_gain: float32 [2048], replicated, may hold values from 0.1 to 1.9
- query_weight: bfloat16 [2048, 8192], P(None, 'tp'), may hold values from -4 to 4
- key_weight: bfloat16 [2048, 2048], P(None, 'tp'), may hold values from -1 to 1
- value_projection_weight: bfloat16 [2048, 2048], P(None, 'tp'), may hold values from -0.125 to 0.125
- output_weight: bfloat16 [8192, 2048], P('tp'), may hold values from -0.0625 to 0.0625
Outputs:
- target_grad: float32 [512, 2048], P(('sp', 'tp'))
- source_grad: float32 [1024, 2048], P(('sp', 'tp'))
- key_weight_grad: float32 [2048, 2048], P(None, 'tp')
All inputs are finite; a program needn't handle non-finite values.
Results may differ from a plain program's by a relative error of at most 0.018.
The roundings to bfloat16 on the way count: a program that leaves them out, or rounds other values in their place, can miss the bound.
Values may be sent and summed in bfloat16 or wider, within the bound.
A program may use at most 64 MiB of HBM per device.

v0:
```python
import jax
import jax.numpy as jnp
from jax import lax
from jax.sharding import PartitionSpec as P

HEAD_SIZE = 256
EPSILON = 1e-05


def as_sent(array):

    def short(part):
        return part.astype(jnp.bfloat16) if part.dtype == jnp.float32 else part

    return jax.tree.map(short, array)


def partner_2(value, axis, bit):
    mask = 2**bit
    pairs = [(source, source ^ mask) for source in range(lax.axis_size(axis))]
    return lax.ppermute(value, axis, pairs)


def combined_all(value, axis, join):
    pieces = jax.tree.map(lambda part: lax.all_gather(part, axis), value)
    head = jax.tree.map(lambda part: part[0], pieces)
    tail = jax.tree.map(lambda part: part[1:], pieces)
    running, _ = lax.scan(lambda running, piece: (join(running, piece), None), head, tail)
    return running


def norm_rows(rows):
    values = rows.astype(jnp.float32)
    centred = values - jnp.mean(values, axis=-1, keepdims=True)
    inverse = lax.rsqrt(jnp.mean(centred * centred, axis=-1, keepdims=True) + EPSILON)
    return (centred * inverse, inverse)


def norm_back(scaled, inverse, gain, upstream):
    weighted = upstream * gain
    spread = jnp.mean(weighted * scaled, axis=-1, keepdims=True)
    return inverse * (weighted - jnp.mean(weighted, axis=-1, keepdims=True) - scaled * spread)


def times_transposed(left, right):
    return lax.dot_general(
        left, right, (((1,), (1,)), ((), ())), preferred_element_type=jnp.float32
    )


def split_heads(flat):
    return flat.reshape(flat.shape[0], flat.shape[1] // HEAD_SIZE, HEAD_SIZE)


def head_scores(queries, key_rows):
    return jnp.einsum(
        "rhd,sd->hrs", queries, key_rows, preferred_element_type=jnp.float32
    ) * HEAD_SIZE ** (-0.5)


def block_statistics(queries, out_grads, key_rows, value_rows):
    scores = head_scores(queries, key_rows)
    highest = jnp.max(scores, axis=2)
    weights = jnp.exp(scores - highest[:, :, None])
    products = jnp.einsum("rhd,sd->hrs", out_grads, value_rows, preferred_element_type=jnp.float32)
    return (highest, jnp.sum(weights, axis=2), jnp.sum(weights * products, axis=2))


def combine_statistics(former, latter):
    highest = jnp.maximum(former[0], latter[0])
    early_scale = jnp.exp(former[0] - highest)
    late_scale = jnp.exp(latter[0] - highest)
    return (
        highest,
        former[1] * early_scale + latter[1] * late_scale,
        former[2] * early_scale + latter[2] * late_scale,
    )


def score_grads(queries, out_grads, key_rows, value_rows, log_total, drifts):
    scores = head_scores(queries, key_rows)
    softmax_weights = jnp.exp(scores - log_total[:, :, None])
    products = jnp.einsum("rhd,sd->hrs", out_grads, value_rows, preferred_element_type=jnp.float32)
    slopes = (softmax_weights * (products - drifts[:, :, None]) * HEAD_SIZE ** (-0.5)).astype(
        jnp.bfloat16
    )
    return (softmax_weights.astype(jnp.bfloat16), slopes)


def join_heads(stacked):
    position = lax.axis_index("tp")
    part_cols = stacked.shape[2]
    bit_level = 0
    while part_cols < HEAD_SIZE:
        partner = jax.tree.map(
            lambda part, own: part.astype(own.dtype),
            partner_2(as_sent(stacked), "tp", bit_level),
            stacked,
        )
        upper_half = position >> bit_level & 1
        stacked = jnp.where(
            upper_half == 0,
            jnp.concatenate((stacked, partner), 2),
            jnp.concatenate((partner, stacked), 2),
        )
        part_cols = part_cols * 2
        bit_level = bit_level + 1
    return stacked


def split_sums(stacked, part_cols):
    position = lax.axis_index("tp")
    bit_count = (HEAD_SIZE // part_cols).bit_length() - 1
    for bit_level in reversed(range(bit_count)):
        half_cols = stacked.shape[2] // 2
        lower_half = stacked[:, :, :half_cols]
        upper_cols = stacked[:, :, half_cols:]
        upper_half = position >> bit_level & 1
        kept_half = jnp.where(upper_half == 0, lower_half, upper_cols)
        sent_half = jnp.where(upper_half == 0, upper_cols, lower_half)
        stacked = kept_half + partner_2(sent_half, "tp", bit_level)
    return stacked


def on_device(
    target,
    source,
    cotangent,
    target_gain,
    source_gain,
    query_weight,
    key_weight,
    value_projection_weight,
    output_weight,
):
    part_cols = key_weight.shape[1]
    src_scaled, src_inverse = norm_rows(source)
    src_normed = (src_scaled * source_gain).astype(jnp.bfloat16)
    tgt_scaled, tgt_inverse = norm_rows(target)
    tgt_normed = (tgt_scaled * target_gain).astype(jnp.bfloat16)
    block_rows = lax.all_gather(src_normed, "tp", axis=0, tiled=True)
    key_portion = jnp.dot(block_rows, key_weight, preferred_element_type=jnp.float32).astype(
        jnp.bfloat16
    )
    value_part = jnp.dot(
        block_rows, value_projection_weight, preferred_element_type=jnp.float32
    ).astype(jnp.bfloat16)
    parted = jnp.stack((key_portion, value_part))
    queries = split_heads(
        jnp.dot(tgt_normed, query_weight, preferred_element_type=jnp.float32).astype(jnp.bfloat16)
    )
    out_grads = split_heads(times_transposed(cotangent, output_weight).astype(jnp.bfloat16))
    head_count = queries.shape[1]
    own_rows = queries.shape[0]
    own_keys = join_heads(parted)
    all_queries, all_grads = (
        lax.all_gather(queries, "sp", axis=0, tiled=True),
        lax.all_gather(out_grads, "sp", axis=0, tiled=True),
    )
    partial_value = block_statistics(all_queries, all_grads, own_keys[0], own_keys[1])
    highest, totals, weighted = combined_all(partial_value, "sp", combine_statistics)
    log_total = highest + jnp.log(totals)
    drifts = weighted / totals
    attention, slopes = score_grads(
        all_queries, all_grads, own_keys[0], own_keys[1], log_total, drifts
    )
    key_gradient_rows = jnp.einsum(
        "hrs,rhd->sd", slopes, all_queries, preferred_element_type=jnp.float32
    )
    value_gradient_rows = jnp.einsum(
        "hrs,rhd->sd", attention, all_grads, preferred_element_type=jnp.float32
    )
    row_start = lax.axis_index("sp") * own_rows
    own_log = lax.dynamic_slice_in_dim(log_total, row_start, own_rows, 1)
    own_drifts = lax.dynamic_slice_in_dim(drifts, row_start, own_rows, 1)
    pieces = lax.all_gather(own_keys, "sp", axis=1, tiled=True)
    unused, slopes = score_grads(queries, out_grads, pieces[0], pieces[1], own_log, own_drifts)
    query_grads = jnp.einsum("hrs,sd->rhd", slopes, pieces[0], preferred_element_type=jnp.float32)
    summed = split_sums(jnp.stack((key_gradient_rows, value_gradient_rows)), part_cols)
    key_flattened = summed[0].astype(jnp.bfloat16)
    value_flattened = summed[1].astype(jnp.bfloat16)
    weight_part = lax.dot_general(
        block_rows, key_flattened, (((0,), (0,)), ((), ())), preferred_element_type=jnp.float32
    )
    key_weight_grad = lax.psum(weight_part.astype(jnp.bfloat16), "sp").astype(jnp.float32)
    source_upstream = lax.psum_scatter(
        (
            times_transposed(key_flattened, key_weight)
            + times_transposed(value_flattened, value_projection_weight)
        ).astype(jnp.bfloat16),
        "tp",
        scatter_dimension=0,
        tiled=True,
    ).astype(jnp.float32)
    source_grad = norm_back(src_scaled, src_inverse, source_gain, source_upstream)
    query_flat = query_grads.astype(jnp.bfloat16).reshape(own_rows, head_count * HEAD_SIZE)
    out_rows = own_rows // lax.axis_size("tp")
    out_start = lax.axis_index("tp") * out_rows
    target_upstream = lax.psum_scatter(
        times_transposed(query_flat, query_weight), "tp", scatter_dimension=0, tiled=True
    )
    slice_scaled = lax.dynamic_slice_in_dim(tgt_scaled, out_start, out_rows, 0)
    slice_inverse = lax.dynamic_slice_in_dim(tgt_inverse, out_start, out_rows, 0)
    slice_cotangent = lax.dynamic_slice_in_dim(cotangent, out_start, out_rows, 0)
    target_grad = slice_cotangent.astype(jnp.float32) + norm_back(
        slice_scaled, slice_inverse, target_gain, target_upstream
    )
    return (target_grad, source_grad, key_weight_grad)


def solution(mesh):
    return jax.shard_map(
        on_device,
        mesh=mesh,
        in_specs=(
            P("sp", None),
            P(("sp", "tp"), None),
            P("sp", None),
            P(),
            P(),
            P(None, "tp"),
            P(None, "tp"),
            P(None, "tp"),
            P("tp", None),
        ),
        out_specs=(P(("sp", "tp"), None), P(("sp", "tp"), None), P(None, "tp")),
        check_vma=False,
    )
```

profile of v0, /device:TPU:0, one launch (start us, length us, event | category | flops | bytes accessed | tf_op | source)
XLA Modules:
  0.0 308.4 jit_solution(17943720126214287300)
XLA Ops:
  7.2 0.0 all-gather.11.cloned.1.call-start
  7.2 1.1 convert_reduce_fusion.1
  8.3 1.1 fusion.46
  9.5 1.7 fusion.42
  11.2 0.0 all-gather.15.cloned.1.call-start
  11.2 1.2 convert_reduce_fusion
  12.4 1.3 fusion.22
  13.8 3.2 %convolution_convert_fusion.2 = bf16[128,1024]{1,0:T(8,128)(2,1)S(1)} fusion(bf16[2048,1024]{1,0:T(8,128)(2,1)} %param.16, f32[2048]{0:T(1024)} %param.14, bf16[128,2048]{1,0:T(8,128)(2,1)} %param.11, f32[128]{0:T(128)S(1)} %add_rsqrt_fusion.1, f32[128]{0:T(128)S(1)} %broadcast_multiply_fusion.5), kind=kOutput, calls=%fused_computation.38 | convolution fusion | flops 538312704 | bytes 4989952 | tf_op jit(solution)/shard_map/dot_general | solution.py:150
  17.0 0.7 copy-done.8
  17.7 0.7 copy.30
  18.4 0.0 all-gather.17.cloned.1.call-start
  18.5 3.7 %convolution_convert_fusion.1 = bf16[128,1024]{1,0:T(8,128)(2,1)S(1)} fusion(bf16[128,2048]{1,0:T(8,128)(2,1)S(1)} %copy-done.9, bf16[1024,2048]{1,0:T(8,128)(2,1)} %param.19), kind=kOutput, calls=%fused_computation.37 | convolution fusion | flops 537001984 | bytes 4980736 | tf_op jit(solution)/shard_map/dot_general | solution.py:46
  22.2 0.7 copy-done.6
  22.9 0.7 copy.29
  23.7 0.0 all-gather.13.cloned.1.call-start
  23.7 13.7 %all-gather.11.cloned.1.call-done = bf16[256,2048]{1,0:T(8,128)(2,1)} async-done(((bf16[32,2048]{1,0:T(8,128)(2,1)}), bf16[256,2048]{1,0:T(8,128)(2,1)}) %all-gather.11.cloned.1.call-update) | async-done | bytes 1048592 | tf_op jit(solution)/shard_map/all_gather | solution.py:141
  37.4 1.7 convolution_convert_fusion.4
  39.2 0.4 convolution_convert_fusion.3
  39.7 27.9 %all-gather.15.cloned.1.call-done = bf16[512,4,256]{2,0,1:T(8,128)(2,1)} async-done(((bf16[128,4,256]{2,0,1:T(8,128)(2,1)}), bf16[512,4,256]{2,0,1:T(8,128)(2,1)}) %all-gather.15.cloned.1.call-update) | async-done | bytes 1048592 | tf_op jit(solution)/shard_map/all_gather | solution.py:157
  67.6 1.7 bitcast_reduce_fusion
  69.3 27.8 %all-gather.17.cloned.1.call-done = bf16[512,4,256]{2,0,1:T(8,128)(2,1)} async-done(((bf16[128,4,256]{2,0,1:T(8,128)(2,1)}), bf16[512,4,256]{2,0,1:T(8,128)(2,1)}) %all-gather.17.cloned.1.call-update) | async-done | bytes 1048592 | tf_op jit(solution)/shard_map/all_gather | solution.py:158
  97.1 3.1 fusion.7
  100.2 13.1 %all-gather.5 = f32[4,4,512]{2,1,0:T(4,128)S(1)} all-gather(f32[1,4,512]{2,1,0:T(4,128)S(1)} %bitcast.163), channel_id=4, replica_groups=mesh['sp'=4,'tp'=8] {'sp'}, dimensions={0}, use_global_device_ids=true | all-gather | bytes 40960 | tf_op jit(solution)/shard_map/all_gather | solution.py:25
  113.3 13.1 %all-gather.4 = f32[4,4,512]{2,1,0:T(4,128)S(1)} all-gather(f32[1,4,512]{2,1,0:T(4,128)S(1)} %bitcast.162), channel_id=3, replica_groups=mesh['sp'=4,'tp'=8] {'sp'}, dimensions={0}, use_global_device_ids=true | all-gather | bytes 40960 | tf_op jit(solution)/shard_map/all_gather | solution.py:25
  126.5 13.1 %all-gather.3 = f32[4,4,512]{2,1,0:T(4,128)S(1)} all-gather(f32[1,4,512]{2,1,0:T(4,128)S(1)} %bitcast.161), channel_id=2, replica_groups=mesh['sp'=4,'tp'=8] {'sp'}, dimensions={0}, use_global_device_ids=true | all-gather | bytes 40960 | tf_op jit(solution)/shard_map/all_gather | solution.py:25
  139.6 0.7 pad_maximum_fusion
  140.4 0.0 all-reduce.2.cloned.1.call-start
  140.4 0.3 while.14
  140.7 2.5 fusion.20
  143.3 1.5 convolution_convert_fusion
  144.8 0.0 reduce-scatter.5.cloned.1.call-start
  144.8 1.8 fusion.55
  146.6 4.6 %fusion.3 = bf16[256,2048]{1,0:T(8,128)(2,1)} fusion(f32[256,2048]{1,0:T(8,128)} %fusion.55, bf16[2048,256]{1,0:T(8,128)(2,1)} %param.18, bf16[512,4,256]{2,0,1:T(8,128)(2,1)} %all-gather.17.cloned.1.call-done, f32[256,512,4]{1,0,2:T(8,128)S(1)} %get-tuple-element.70, f32[4,512]{1,0:T(4,128)S(1)} %get-tuple-element.67), kind=kOutput, calls=%fused_computation.9 | convolution fusion | flops 539033600 | bytes 7348224 | tf_op jit(solution)/shard_map/dot_general | solution.py:46
  151.2 0.0 reduce-scatter.3.cloned.1.call-start
  151.3 16.6 %all-gather.13.cloned.1.call-done = bf16[2,1024,256]{2,1,0:T(8,128)(2,1)} async-done(((bf16[2,256,256]{2,1,0:T(8,128)(2,1)}), bf16[2,1024,256]{2,1,0:T(8,128)(2,1)}) %all-gather.13.cloned.1.call-update) | async-done | bytes 1048592 | tf_op jit(solution)/shard_map/all_gather | solution.py:176
  167.9 1.6 fusion.36
  169.5 2.9 fusion.19
  172.4 4.8 %fusion.54 = f32[128,2048]{1,0:T(8,128)} fusion(bf16[128,1024]{0,1:T(8,128)(2,1)} %bitcast.160, bf16[2048,1024]{1,0:T(8,128)(2,1)} %param.16), kind=kOutput, calls=%fused_computation.98 | convolution fusion | flops 536870912 | bytes 5505024 | tf_op jit(solution)/shard_map/dot_general | solution.py:46
  177.2 0.1 dynamic-slice.3
  177.3 0.3 fusion.17
  177.7 43.8 %all-reduce.2.cloned.1.call-done = bf16[2048,256]{1,0:T(8,128)(2,1)} async-done(((bf16[2048,256]{1,0:T(8,128)(2,1)}), bf16[2048,256]{1,0:T(8,128)(2,1)}) %all-reduce.2.cloned.1.call-update) | async-done | bytes 1048592 | tf_op jit(solution)/shard_map/psum | solution.py:185
  221.4 2.7 convert_element_type.79
  224.1 35.6 %reduce-scatter.5.cloned.1.call-done = bf16[32,2048]{1,0:T(8,128)(2,1)} async-done(((bf16[256,2048]{1,0:T(8,128)(2,1)}), bf16[32,2048]{1,0:T(8,128)(2,1)}) %reduce-scatter.5.cloned.1.call-update) | async-done | bytes 131088 | tf_op jit(solution)/shard_map/reduce_scatter | solution.py:186
  259.7 1.1 fusion.47
  260.9 1.7 fusion.45
  262.6 36.3 %reduce-scatter.3.cloned.1.call-done = f32[16,2048]{1,0:T(8,128)} async-done(((f32[128,2048]{1,0:T(8,128)}), f32[16,2048]{1,0:T(8,128)}) %reduce-scatter.3.cloned.1.call-update) | async-done | bytes 131088 | tf_op jit(solution)/shard_map/reduce_scatter | solution.py:199
  298.9 1.0 multiply_reduce_fusion.1
  299.9 1.7 multiply_add_fusion
  (53 shorter events, 0.4 us)
Async XLA Ops:
  7.2 30.3 %copy-start = (bf16[2048,256]{1,0:T(8,128)(2,1)S(1)}, bf16[2048,256]{1,0:T(8,128)(2,1)}, u32[]{:S(2)}) copy-start(bf16[2048,256]{1,0:T(8,128)(2,1)} %param.17) | copy-start | bytes 3145732
  7.2 30.2 %all-gather.11.cloned.1.call-start = ((), (), s32[]{:S(2)}) async-start(), calls=%async_computation.2 | async-start | bytes 1179648 | tf_op jit(solution)/shard_map/all_gather | solution.py:141
  11.2 56.4 %all-gather.15.cloned.1.call-start = ((), (), s32[]{:S(2)}) async-start(), calls=%async_computation.4 | async-start | bytes 1310720 | tf_op jit(solution)/shard_map/all_gather | solution.py:157
  13.8 4.7 %copy-start.9 = (bf16[128,2048]{1,0:T(8,128)(2,1)S(1)}, bf16[128,2048]{1,0:T(8,128)(2,1)}, u32[]{:S(2)}) copy-start(bf16[128,2048]{1,0:T(8,128)(2,1)} %param.13) | copy-start | bytes 1572868
  17.0 0.7 copy-start.8
  18.4 78.7 %all-gather.17.cloned.1.call-start = ((), (), s32[]{:S(2)}) async-start(), calls=%async_computation.5 | async-start | bytes 1310720 | tf_op jit(solution)/shard_map/all_gather | solution.py:158
  22.2 0.7 copy-start.6
  22.2 17.0 %copy-start.4 = (bf16[2048,256]{1,0:T(8,128)(2,1)S(1)}, bf16[2048,256]{1,0:T(8,128)(2,1)}, u32[]{:S(2)}) copy-start(bf16[2048,256]{1,0:T(8,128)(2,1)} %param.18) | copy-start | bytes 3145732
  23.7 144.2 %all-gather.13.cloned.1.call-start = ((), (), s32[]{:S(2)}) async-start(), calls=%async_computation.3 | async-start | bytes 1310720 | tf_op jit(solution)/shard_map/all_gather | solution.py:176
  37.4 1.8 copy-start.1
  140.4 81.1 %all-reduce.2.cloned.1.call-start = ((), (), s32[]{:S(2)}) async-start(), calls=%async_computation.8 | async-start | bytes 2097152 | tf_op jit(solution)/shard_map/psum | solution.py:185
  140.7 2.6 copy-start.2
  144.8 115.0 %reduce-scatter.5.cloned.1.call-start = ((), (), s32[]{:S(2)}) async-start(), calls=%async_computation.7 | async-start | bytes 1179648 | tf_op jit(solution)/shard_map/reduce_scatter | solution.py:186
  151.2 18.2 %copy-start.7 = (bf16[128,1024]{1,0:T(8,128)(2,1)S(1)}, bf16[128,1024]{1,0:T(8,128)(2,1)}, u32[]{:S(2)}) copy-start(bf16[128,1024]{1,0:T(8,128)(2,1)} %copy-done.6) | copy-start | bytes 786436
  151.2 147.6 %reduce-scatter.3.cloned.1.call-start = ((), (), s32[]{:S(2)}) async-start(), calls=%async_computation.6 | async-start | bytes 1179648 | tf_op jit(solution)/shard_map/reduce_scatter | solution.py:199
  172.4 5.0 %copy-start.3 = (bf16[128,2048]{1,0:T(8,128)(2,1)S(1)}, bf16[128,2048]{1,0:T(8,128)(2,1)}, u32[]{:S(2)}) copy-start(bf16[128,2048]{1,0:T(8,128)(2,1)} %param.11) | copy-start | bytes 1572868
  177.3 82.4 %copy-start.5 = (bf16[32,2048]{1,0:T(8,128)(2,1)S(1)}, bf16[32,2048]{1,0:T(8,128)(2,1)}, u32[]{:S(2)}) copy-start(bf16[32,2048]{1,0:T(8,128)(2,1)} %param.12) | copy-start | bytes 393220
  177.3 82.4 %copy-start.10 = (f32[2048]{0:T(1024)S(1)}, f32[2048]{0:T(1024)}, u32[]{:S(2)}) copy-start(f32[2048]{0:T(1024)} %param.15) | copy-start | bytes 24580
  177.6 121.2 %copy-start.11 = (f32[2048]{0:T(1024)S(1)}, f32[2048]{0:T(1024)}, u32[]{:S(2)}) copy-start(f32[2048]{0:T(1024)} %param.14) | copy-start | bytes 24580
Sparse Core Ops, SparseCore 0:
  11.3 26.0 all-gather.10
  39.6 27.9 all-gather.14
  69.7 27.3 all-gather.16
  140.5 27.3 all-gather.12
  170.1 51.2 all-reduce.1
  224.4 35.2 reduce-scatter.4
  262.9 35.9 reduce-scatter.2
where the time goes:
time: 309 us; the launch traced here: 308 us
  waiting for transfers between devices  202 us (65%)
  blocking collectives  39.4 us (13%)
  matrix products  33.6 us (11%)
  other arithmetic  16 us (5%)
  between operations  14.3 us (5%)
    psum x1, waiting for transfers between devices, on_device(): lax.psum(weight_part.astype(jnp.bfloat16), 'sp').astype(jnp.float32)  43.8 us
    all_gather x3, blocking collectives, combined_all(): pieces = jax.tree.map(lambda part: lax.all_gather(part, axis), value)  39.4 us
    reduce_scatter x1, waiting for transfers between devices, on_device(): lax.psum_scatter(times_transposed(query_flat, query_weight), 'tp', scatte...  36.3 us
    reduce_scatter x1, waiting for transfers between devices, on_device(): lax.psum_scatter((times_transposed(key_flattened, key_weight) + times_tra...  35.6 us
    all_gather x1, waiting for transfers between devices, on_device(): lax.all_gather(queries, 'sp', axis=0, tiled=True)  27.9 us
    all_gather x1, waiting for transfers between devices, on_device(): lax.all_gather(out_grads, 'sp', axis=0, tiled=True)  27.8 us
    all_gather x1, waiting for transfers between devices, on_device(): pieces = lax.all_gather(own_keys, 'sp', axis=1, tiled=True)  16.6 us
    dot_general x4, matrix products, times_transposed(): lax.dot_general(left, right, (((1,), (1,)), ((), ())), preferred_element_...  15 us
  transfers between devices with their start and end apart: 7, of which 7 were waited for; matrix products, arithmetic and copies ran while one was open for 13% of the time, Pallas kernels for 0%

commit v1 on v0

--- a/solution.py
+++ b/solution.py
@@ -173,7 +173,14 @@
     row_start = lax.axis_index("sp") * own_rows
     own_log = lax.dynamic_slice_in_dim(log_total, row_start, own_rows, 1)
     own_drifts = lax.dynamic_slice_in_dim(drifts, row_start, own_rows, 1)
-    pieces = lax.all_gather(own_keys, "sp", axis=1, tiled=True)
+    count = lax.axis_size("sp")
+    forward = [(i, (i + 1) % count) for i in range(count)]
+    parts = [own_keys]
+    for hop in range(1, count):
+        parts = [lax.ppermute(parts[0], "sp", forward), *parts]
+    whole = jnp.concatenate(parts, axis=1)
+    offset = (lax.axis_index("sp") + 1) * parts[-1].shape[1]
+    pieces = jnp.roll(whole, offset, axis=1)
     unused, slopes = score_grads(queries, out_grads, pieces[0], pieces[1], own_log, own_drifts)
     query_grads = jnp.einsum("hrs,sd->rhd", slopes, pieces[0], preferred_element_type=jnp.float32)
     summed = split_sums(jnp.stack((key_gradient_rows, value_gradient_rows)), part_cols)

time: 309 us -> 289 us (0.935)
  waiting for transfers between devices: 202 us -> 178 us
  local copies, waits for them, and re-layouts: 3.01 us -> 8.38 us
    psum x1, waiting for transfers between devices: 43.8 us -> 7.68 us  [on_device(): lax.psum(weight_part.astype(jnp.bfloat16), 'sp').astype(jnp.float32)]
    ppermute x0 -> x3, waiting for transfers between devices: none -> 27.9 us  [on_device(): parts = [lax.ppermute(parts[0], 'sp', forward), *parts]]
    all_gather x1 -> x0, waiting for transfers between devices: 16.6 us -> none  [on_device(): pieces = lax.all_gather(own_keys, 'sp', axis=1, tiled=True)]
    unnamed x24 -> x48, local copies, waits for them, and re-layouts: 1.46 us -> 6.77 us
  transfers between devices with their start and end apart: 7 -> 9, of which waited for: 7 -> 9; matrix products, arithmetic and copies ran while one was open for 13% -> 14% of each run, Pallas kernels for 0% -> 0%
where the time goes in v1:
time: 289 us; the launch traced here: 288 us
  waiting for transfers between devices  178 us (62%)
  blocking collectives  39.4 us (14%)
  matrix products  31.7 us (11%)
  other arithmetic  16 us (6%)
  between operations  14.5 us (5%)
  local copies, waits for them, and re-layouts  8.38 us (3%)
    all_gather x3, blocking collectives, combined_all(): pieces = jax.tree.map(lambda part: lax.all_gather(part, axis), value)  39.4 us
    reduce_scatter x1, waiting for transfers between devices, on_device(): lax.psum_scatter(times_transposed(query_flat, query_weight), 'tp', scatte...  36.1 us
    reduce_scatter x1, waiting for transfers between devices, on_device(): lax.psum_scatter((times_transposed(key_flattened, key_weight) + times_tra...  35.6 us
    all_gather x1, waiting for transfers between devices, on_device(): lax.all_gather(queries, 'sp', axis=0, tiled=True)  27.9 us
    ppermute x3, waiting for transfers between devices, on_device(): parts = [lax.ppermute(parts[0], 'sp', forward), *parts]  27.9 us
    all_gather x1, waiting for transfers between devices, on_device(): lax.all_gather(out_grads, 'sp', axis=0, tiled=True)  27.8 us
    all_gather x1, waiting for transfers between devices, on_device(): block_rows = lax.all_gather(src_normed, 'tp', axis=0, tiled=True)  15 us
    dot_general x4, matrix products, times_transposed(): lax.dot_general(left, right, (((1,), (1,)), ((), ())), preferred_element_...  14.8 us
  transfers between devices with their start and end apart: 9, of which 9 were waited for; matrix products, arithmetic and copies ran while one was open for 14% of the time, Pallas kernels for 0%

profile of v1, /device:TPU:0, one launch (start us, length us, event | category | flops | bytes accessed | tf_op | source)
XLA Modules:
  0.0 288.4 jit_solution(16550787706448440743)
XLA Ops:
  7.2 1.1 convert_reduce_fusion.1
  8.4 1.1 fusion.46
  9.5 1.7 fusion.42
  11.2 1.2 convert_reduce_fusion
  12.4 1.3 fusion.22
  13.8 3.2 %convolution_convert_fusion.2 = bf16[128,1024]{1,0:T(8,128)(2,1)S(1)} fusion(bf16[2048,1024]{1,0:T(8,128)(2,1)} %param.16, f32[2048]{0:T(1024)} %param.14, bf16[128,2048]{1,0:T(8,128)(2,1)} %param.11, f32[128]{0:T(128)S(1)} %add_rsqrt_fusion.1, f32[128]{0:T(128)S(1)} %broadcast_multiply_fusion.5), kind=kOutput, calls=%fused_computation.38 | convolution fusion | flops 538312704 | bytes 4989952 | tf_op jit(solution)/shard_map/dot_general | solution.py:150
  17.0 0.8 copy.30
  17.9 3.7 %convolution_convert_fusion.1 = bf16[128,1024]{1,0:T(8,128)(2,1)S(1)} fusion(bf16[128,2048]{1,0:T(8,128)(2,1)S(1)} %copy-done.9, bf16[1024,2048]{1,0:T(8,128)(2,1)} %param.19), kind=kOutput, calls=%fused_computation.37 | convolution fusion | flops 537001984 | bytes 4980736 | tf_op jit(solution)/shard_map/dot_general | solution.py:46
  21.6 0.7 copy.29
  22.4 15.0 %all-gather.10.cloned.1.call-done = bf16[256,2048]{1,0:T(8,128)(2,1)} async-done(((bf16[32,2048]{1,0:T(8,128)(2,1)}), bf16[256,2048]{1,0:T(8,128)(2,1)}) %all-gather.10.cloned.1.call-update) | async-done | bytes 1048592 | tf_op jit(solution)/shard_map/all_gather | solution.py:141
  37.4 1.8 convolution_convert_fusion.4
  39.2 0.4 convolution_convert_fusion.3
  39.7 27.9 %all-gather.12.cloned.1.call-done = bf16[512,4,256]{2,0,1:T(8,128)(2,1)} async-done(((bf16[128,4,256]{2,0,1:T(8,128)(2,1)}), bf16[512,4,256]{2,0,1:T(8,128)(2,1)}) %all-gather.12.cloned.1.call-update) | async-done | bytes 1048592 | tf_op jit(solution)/shard_map/all_gather | solution.py:157
  67.6 1.7 bitcast_reduce_fusion
  69.3 27.8 %all-gather.14.cloned.1.call-done = bf16[512,4,256]{2,0,1:T(8,128)(2,1)} async-done(((bf16[128,4,256]{2,0,1:T(8,128)(2,1)}), bf16[512,4,256]{2,0,1:T(8,128)(2,1)}) %all-gather.14.cloned.1.call-update) | async-done | bytes 1048592 | tf_op jit(solution)/shard_map/all_gather | solution.py:158
  97.1 3.1 %fusion.7 = (f32[4,512]{1,0:T(4,128)S(1)}, f32[4,512]{1,0:T(4,128)S(1)}, f32[256,512,4]{1,0,2:T(8,128)}) fusion(f32[256,512,4]{1,0,2:T(8,128)S(1)} %get-tuple-element.70, f32[4,512]{1,0:T(4,128)S(1)} %get-tuple-element.69, bf16[512,4,256]{2,0,1:T(8,128)(2,1)} %all-gather.14.cloned.1.call-done, bf16[256,256]{1,0:T(8,128)(2,1)S(1)} %convolution_convert_fusion.3), kind=kOutput, calls=%fused_computation.17 | convolution fusion | flops 270528512 | bytes 5398528 | tf_op jit(solution)/shard_map/rhd,sd->hrs/dot_general | solution.py:65
  100.2 13.1 %all-gather.5 = f32[4,4,512]{2,1,0:T(4,128)S(1)} all-gather(f32[1,4,512]{2,1,0:T(4,128)S(1)} %bitcast.167), channel_id=4, replica_groups=mesh['sp'=4,'tp'=8] {'sp'}, dimensions={0}, use_global_device_ids=true | all-gather | bytes 40960 | tf_op jit(solution)/shard_map/all_gather | solution.py:25
  113.3 13.1 %all-gather.4 = f32[4,4,512]{2,1,0:T(4,128)S(1)} all-gather(f32[1,4,512]{2,1,0:T(4,128)S(1)} %bitcast.166), channel_id=3, replica_groups=mesh['sp'=4,'tp'=8] {'sp'}, dimensions={0}, use_global_device_ids=true | all-gather | bytes 40960 | tf_op jit(solution)/shard_map/all_gather | solution.py:25
  126.5 13.1 %all-gather.3 = f32[4,4,512]{2,1,0:T(4,128)S(1)} all-gather(f32[1,4,512]{2,1,0:T(4,128)S(1)} %bitcast.165), channel_id=2, replica_groups=mesh['sp'=4,'tp'=8] {'sp'}, dimensions={0}, use_global_device_ids=true | all-gather | bytes 40960 | tf_op jit(solution)/shard_map/all_gather | solution.py:25
  139.6 0.3 while.14
  139.9 2.5 fusion.20
  142.5 1.5 convolution_convert_fusion
  144.0 0.7 pad_maximum_fusion
  144.7 9.3 %collective-permute-done = bf16[2,256,256]{2,1,0:T(8,128)(2,1)} collective-permute-done((bf16[2,256,256]{2,1,0:T(8,128)(2,1)}, bf16[2,256,256]{2,1,0:T(8,128)(2,1)}, u32[]{:S(2)}, u32[]{:S(2)}) %collective-permute-start) | collective-permute-done | bytes 262176 | tf_op jit(solution)/shard_map/ppermute | solution.py:180
  154.0 1.8 fusion.58
  155.8 13.5 %collective-permute-done.1 = bf16[2,256,256]{2,1,0:T(8,128)(2,1)} collective-permute-done((bf16[2,256,256]{2,1,0:T(8,128)(2,1)}, bf16[2,256,256]{2,1,0:T(8,128)(2,1)}, u32[]{:S(2)}, u32[]{:S(2)}) %collective-permute-start.1) | collective-permute-done | bytes 262176 | tf_op jit(solution)/shard_map/ppermute | solution.py:180
  169.3 4.5 %fusion.3 = bf16[256,2048]{1,0:T(8,128)(2,1)} fusion(f32[256,2048]{1,0:T(8,128)} %fusion.58, bf16[2048,256]{1,0:T(8,128)(2,1)} %param.18, bf16[512,4,256]{2,0,1:T(8,128)(2,1)} %all-gather.14.cloned.1.call-done, f32[256,512,4]{1,0,2:T(8,128)S(1)} %get-tuple-element.70, f32[4,512]{1,0:T(4,128)S(1)} %get-tuple-element.67), kind=kOutput, calls=%fused_computation.9 | convolution fusion | flops 539033600 | bytes 7348224 | tf_op jit(solution)/shard_map/dot_general | solution.py:46
  174.0 5.1 %collective-permute-done.2 = bf16[2,256,256]{2,1,0:T(8,128)(2,1)} collective-permute-done((bf16[2,256,256]{2,1,0:T(8,128)(2,1)}, bf16[2,256,256]{2,1,0:T(8,128)(2,1)}, u32[]{:S(2)}, u32[]{:S(2)}) %collective-permute-start.2) | collective-permute-done | bytes 262176 | tf_op jit(solution)/shard_map/ppermute | solution.py:180
  179.0 1.0 constant_dynamic-update-slice_fusion.7
  180.0 1.0 constant_dynamic-update-slice_fusion.6
  181.0 1.0 constant_dynamic-update-slice_fusion.5
  182.0 1.0 constant_dynamic-update-slice_fusion.3
  183.0 1.0 constant_dynamic-update-slice_fusion.2
  184.0 1.0 constant_dynamic-update-slice_fusion.1
  185.0 0.5 fusion.36
  185.5 0.8 copy-done.10
  186.3 2.3 fusion.19
  188.6 4.8 %fusion.57 = f32[128,2048]{1,0:T(8,128)} fusion(bf16[128,1024]{0,1:T(8,128)(2,1)S(1)} %bitcast.164, bf16[2048,1024]{1,0:T(8,128)(2,1)} %param.16), kind=kOutput, calls=%fused_computation.108 | convolution fusion | flops 536870912 | bytes 5505024 | tf_op jit(solution)/shard_map/dot_general | solution.py:46
  193.4 0.1 dynamic-slice.3
  193.5 0.3 fusion.17
  193.8 7.7 %all-reduce.2.cloned.1.call-done = bf16[2048,256]{1,0:T(8,128)(2,1)} async-done(((bf16[2048,256]{1,0:T(8,128)(2,1)}), bf16[2048,256]{1,0:T(8,128)(2,1)}) %all-reduce.2.cloned.1.call-update) | async-done | bytes 1048592 | tf_op jit(solution)/shard_map/psum | solution.py:192
  201.5 2.7 convert_element_type.79
  204.2 35.6 %reduce-scatter.5.cloned.1.call-done = bf16[32,2048]{1,0:T(8,128)(2,1)} async-done(((bf16[256,2048]{1,0:T(8,128)(2,1)}), bf16[32,2048]{1,0:T(8,128)(2,1)}) %reduce-scatter.5.cloned.1.call-update) | async-done | bytes 131088 | tf_op jit(solution)/shard_map/reduce_scatter | solution.py:193
  239.8 1.1 fusion.47
  241.0 1.7 fusion.45
  242.7 36.1 %reduce-scatter.3.cloned.1.call-done = f32[16,2048]{1,0:T(8,128)} async-done(((f32[128,2048]{1,0:T(8,128)}), f32[16,2048]{1,0:T(8,128)}) %reduce-scatter.3.cloned.1.call-update) | async-done | bytes 131088 | tf_op jit(solution)/shard_map/reduce_scatter | solution.py:206
  278.8 1.0 multiply_reduce_fusion.1
  279.9 1.7 multiply_add_fusion
  (82 shorter events, 0.8 us)
Async XLA Ops:
  7.2 30.3 %copy-start = (bf16[2048,256]{1,0:T(8,128)(2,1)S(1)}, bf16[2048,256]{1,0:T(8,128)(2,1)}, u32[]{:S(2)}) copy-start(bf16[2048,256]{1,0:T(8,128)(2,1)} %param.17) | copy-start | bytes 3145732
  7.2 30.3 %all-gather.10.cloned.1.call-start = ((), (), s32[]{:S(2)}) async-start(), calls=%async_computation.2 | async-start | bytes 1179648 | tf_op jit(solution)/shard_map/all_gather | solution.py:141
  8.3 5.4 %copy-start.13 = (f32[32]{0:T(128)}, f32[32]{0:T(128)S(1)}, u32[]{:S(2)}) copy-start(f32[32]{0:T(128)S(1)} %broadcast_multiply_fusion.4) | copy-start | bytes 388
  9.5 4.3 %copy-start.15 = (f32[32]{0:T(128)}, f32[32]{0:T(128)S(1)}, u32[]{:S(2)}) copy-start(f32[32]{0:T(128)S(1)} %add_rsqrt_fusion) | copy-start | bytes 388
  11.2 56.4 %all-gather.12.cloned.1.call-start = ((), (), s32[]{:S(2)}) async-start(), calls=%async_computation.3 | async-start | bytes 1310720 | tf_op jit(solution)/shard_map/all_gather | solution.py:157
  12.4 4.6 %copy-start.17 = (f32[128]{0:T(128)}, f32[128]{0:T(128)S(1)}, u32[]{:S(2)}) copy-start(f32[128]{0:T(128)S(1)} %broadcast_multiply_fusion.5) | copy-start | bytes 1540
  13.8 3.2 %copy-start.19 = (f32[128]{0:T(128)}, f32[128]{0:T(128)S(1)}, u32[]{:S(2)}) copy-start(f32[128]{0:T(128)S(1)} %add_rsqrt_fusion.1) | copy-start | bytes 1540
  13.8 4.1 %copy-start.9 = (bf16[128,2048]{1,0:T(8,128)(2,1)S(1)}, bf16[128,2048]{1,0:T(8,128)(2,1)}, u32[]{:S(2)}) copy-start(bf16[128,2048]{1,0:T(8,128)(2,1)} %param.13) | copy-start | bytes 1572868
  17.0 4.6 %copy-start.6 = (bf16[128,1024]{1,0:T(8,128)(2,1)}, bf16[128,1024]{1,0:T(8,128)(2,1)S(1)}, u32[]{:S(2)}) copy-start(bf16[128,1024]{1,0:T(8,128)(2,1)S(1)} %convolution_convert_fusion.2) | copy-start | bytes 786436
  17.8 79.3 %all-gather.14.cloned.1.call-start = ((), (), s32[]{:S(2)}) async-start(), calls=%async_computation.4 | async-start | bytes 1310720 | tf_op jit(solution)/shard_map/all_gather | solution.py:158
  21.6 0.8 copy-start.8
  21.6 17.6 %copy-start.4 = (bf16[2048,256]{1,0:T(8,128)(2,1)S(1)}, bf16[2048,256]{1,0:T(8,128)(2,1)}, u32[]{:S(2)}) copy-start(bf16[2048,256]{1,0:T(8,128)(2,1)} %param.18) | copy-start | bytes 3145732
  22.4 179.1 %all-reduce.2.cloned.1.call-start = ((), (), s32[]{:S(2)}) async-start(), calls=%async_computation.7 | async-start | bytes 2097152 | tf_op jit(solution)/shard_map/psum | solution.py:192
  37.4 1.8 copy-start.1
  139.9 2.6 copy-start.2
  144.0 95.8 %reduce-scatter.5.cloned.1.call-start = ((), (), s32[]{:S(2)}) async-start(), calls=%async_computation.6 | async-start | bytes 1179648 | tf_op jit(solution)/shard_map/reduce_scatter | solution.py:193
  144.7 9.3 %collective-permute-start = (bf16[2,256,256]{2,1,0:T(8,128)(2,1)}, bf16[2,256,256]{2,1,0:T(8,128)(2,1)}, u32[]{:S(2)}, u32[]{:S(2)}) collective-permute-start(bf16[2,256,256]{2,1,0:T(8,128)(2,1)} %pad_maximum_fusion), channel_id=1, source_target_pairs={{0,8},{8,16},{16,24},{24,0},{1,9},{9,17},{17,25},{25,1},{2,10},{10... | collective-permute-start | bytes 786440 | tf_op jit(solution)/shard_map/ppermute | solution.py:180
  154.0 15.3 %collective-permute-start.1 = (bf16[2,256,256]{2,1,0:T(8,128)(2,1)}, bf16[2,256,256]{2,1,0:T(8,128)(2,1)}, u32[]{:S(2)}, u32[]{:S(2)}) collective-permute-start(bf16[2,256,256]{2,1,0:T(8,128)(2,1)} %collective-permute-done), channel_id=1, source_target_pairs={{0,8},{8,16},{16,24},{24,0},{1,9},{9,17},{17,25},{25,1},{2,10},{10... | collective-permute-start | bytes 786440 | tf_op jit(solution)/shard_map/ppermute | solution.py:180
  169.3 9.7 %collective-permute-start.2 = (bf16[2,256,256]{2,1,0:T(8,128)(2,1)}, bf16[2,256,256]{2,1,0:T(8,128)(2,1)}, u32[]{:S(2)}, u32[]{:S(2)}) collective-permute-start(bf16[2,256,256]{2,1,0:T(8,128)(2,1)} %collective-permute-done.1), channel_id=1, source_target_pairs={{0,8},{8,16},{16,24},{24,0},{1,9},{9,17},{17,25},{25,1},{2,10},{10... | collective-permute-start | bytes 786440 | tf_op jit(solution)/shard_map/ppermute | solution.py:180
  173.9 105.0 %reduce-scatter.3.cloned.1.call-start = ((), (), s32[]{:S(2)}) async-start(), calls=%async_computation.5 | async-start | bytes 1179648 | tf_op jit(solution)/shard_map/reduce_scatter | solution.py:206
  173.9 11.0 %copy-start.7 = (bf16[128,1024]{1,0:T(8,128)(2,1)S(1)}, bf16[128,1024]{1,0:T(8,128)(2,1)}, u32[]{:S(2)}) copy-start(bf16[128,1024]{1,0:T(8,128)(2,1)} %copy-done.6) | copy-start | bytes 786436
  185.0 1.3 copy-start.10
  188.6 4.8 %copy-start.20 = (f32[128]{0:T(128)S(1)}, f32[128]{0:T(128)}, u32[]{:S(2)}) copy-start(f32[128]{0:T(128)} %copy-done.19) | copy-start | bytes 1540
  188.6 4.9 %copy-start.3 = (bf16[128,2048]{1,0:T(8,128)(2,1)S(1)}, bf16[128,2048]{1,0:T(8,128)(2,1)}, u32[]{:S(2)}) copy-start(bf16[128,2048]{1,0:T(8,128)(2,1)} %param.11) | copy-start | bytes 1572868
  188.6 4.9 %copy-start.18 = (f32[128]{0:T(128)S(1)}, f32[128]{0:T(128)}, u32[]{:S(2)}) copy-start(f32[128]{0:T(128)} %copy-done.17) | copy-start | bytes 1540
  193.5 46.3 %copy-start.5 = (bf16[32,2048]{1,0:T(8,128)(2,1)S(1)}, bf16[32,2048]{1,0:T(8,128)(2,1)}, u32[]{:S(2)}) copy-start(bf16[32,2048]{1,0:T(8,128)(2,1)} %param.12) | copy-start | bytes 393220
  193.5 46.3 %copy-start.11 = (f32[2048]{0:T(1024)S(1)}, f32[2048]{0:T(1024)}, u32[]{:S(2)}) copy-start(f32[2048]{0:T(1024)} %param.15) | copy-start | bytes 24580
  193.5 46.3 %copy-start.14 = (f32[32]{0:T(128)S(1)}, f32[32]{0:T(128)}, u32[]{:S(2)}) copy-start(f32[32]{0:T(128)} %copy-done.13) | copy-start | bytes 388
  193.5 46.3 %copy-start.16 = (f32[32]{0:T(128)S(1)}, f32[32]{0:T(128)}, u32[]{:S(2)}) copy-start(f32[32]{0:T(128)} %copy-done.15) | copy-start | bytes 388
  193.8 85.0 %copy-start.12 = (f32[2048]{0:T(1024)S(1)}, f32[2048]{0:T(1024)}, u32[]{:S(2)}) copy-start(f32[2048]{0:T(1024)} %param.14) | copy-start | bytes 24580
Sparse Core Ops, SparseCore 0:
  11.3 26.0 all-gather.9
  39.6 27.9 all-gather.11
  69.7 27.3 all-gather.13
  144.1 57.3 all-reduce.1
  204.5 35.2 reduce-scatter.4
  242.8 35.9 reduce-scatter.2
